TPU v7x, 32 devices: a whole 2x2x4 slice. The times are simulated.
32 devices in a mesh: sp: 8 (over z, core), tp: 4 (over y, x).
Axes of the slice: x: 2, y: 2, z: 4, core: 2. Of those that a mesh axis runs over, the one named last changes fastest.
Arguments:
- rec_input: bfloat16 [3072, 3072], P('sp', 'tp'), may hold values from -6 to 6
- gate_input: bfloat16 [3072, 3072], P('sp', 'tp'), may hold values from -6 to 6
- conv_weight: bfloat16 [4, 3072], P(None, 'tp'), may hold values from -3 to 3
- decay_wide: bfloat16 [2, 16, 128, 128], P(None, 'tp'), may hold values from -0.5 to 0.5
- decay_narrow: bfloat16 [2, 16, 64, 64], P(None, 'tp'), may hold values from -0.75 to 0.75
- input_wide: bfloat16 [2, 16, 128, 128], P(None, 'tp'), may hold values from -0.5 to 0.5
- input_narrow: bfloat16 [2, 16, 64, 64], P(None, 'tp'), may hold values from -0.75 to 0.75
- decay_base: float32 [2, 3072], P(None, 'tp'), may hold values from 6.510417e-06 to 8.138021e-05
- decay_extra: float32 [2, 3072, 2, 16], P(None, 'sp', None, 'tp'), may hold values from -1 to 0
- tokens: bfloat16 [3072, 2048], P('sp', 'tp'), may hold values from -16 to 16
- out_weight: bfloat16 [3072, 2048], P(None, 'tp'), may hold values from -0.3125 to 0.3125
- norm_gain: float32 [2048], P('tp'), may hold values from 0.1 to 1.9
- shared_gate: bfloat16 [2048, 2048], P(None, 'tp'), may hold values from -0.125 to 0.125
- shared_up: bfloat16 [2048, 2048], P(None, 'tp'), may hold values from -0.125 to 0.125
- shared_down: bfloat16 [2048, 2048], P(None, 'tp'), may hold values from -0.125 to 0.125
- expert_gate: bfloat16 [8, 2048, 2048], P('sp', None, 'tp'), may hold values from -0.125 to 0.125
- expert_up: bfloat16 [8, 2048, 2048], P('sp', None, 'tp'), may hold values from -0.125 to 0.125
- expert_down: bfloat16 [8, 2048, 2048], P('sp', None, 'tp'), may hold values from -0.125 to 0.125
- routes: int32 [3072, 2], P('sp'), may hold values from 0 to 7, all different within a row; in each aligned block of 384 rows (0 to 383, 384 to 767, ...) at most 144 rows name the same one
- route_weight: float32 [3072, 2], P('sp'), may hold values from 0.2 to 1.5
Outputs:
- layer_out: bfloat16 [3072, 2048], P('sp', 'tp')
Inputs may be any that keep to these rules, and one draw needn't show every extreme that they name: `routes`: each row names 2 different experts. The rows of one index of sp name no expert more than 144 times, and in some such block one expert exactly 144 times.
All inputs are finite; a program needn't handle non-finite values.
Results may differ from a plain program's by a relative error of at most 0.0052.
Values may be sent and summed in bfloat16 or wider, within the bound.
A program may use at most 64 MiB of HBM per device.

v0:
```python
import functools

import jax
import jax.numpy as jnp
import numpy as np
from jax import lax
from jax.experimental import pallas as pl
from jax.experimental.pallas import tpu as pltpu
from jax.sharding import PartitionSpec as P

MESH = pl.DeviceIdType.MESH
D = 2048
CONV = 4
NORM_EPS = 1e-06
RATE_SCALE = 8.0
SEG = 8
F32 = jnp.float32
BF16 = jnp.bfloat16
EXACT = lax.Precision.HIGHEST


def rcopy(src, dst, send, recv, **where):
    return pltpu.make_async_remote_copy(
        src_ref=src, dst_ref=dst, send_sem=send, recv_sem=recv, device_id=where, device_id_type=MESH
    )


def greet(n_sp, n_tp):
    sp, tp = lax.axis_index("sp"), lax.axis_index("tp")
    barrier = pltpu.get_barrier_semaphore()
    for k in range(1, n_sp):
        pl.semaphore_signal(
            barrier, inc=1, device_id={"sp": lax.rem(sp + k, n_sp)}, device_id_type=MESH
        )
    for k in range(1, n_tp):
        pl.semaphore_signal(
            barrier, inc=1, device_id={"tp": lax.rem(tp + k, n_tp)}, device_id_type=MESH
        )
    pl.semaphore_wait(barrier, n_sp + n_tp - 2)


def gather_sems(n_tp):
    count = 6 if n_tp == 4 else n_tp
    return [pltpu.SemaphoreType.DMA((count,)), pltpu.SemaphoreType.DMA((count,))]


class Gather:
    def __init__(self, n_tp, slot, send, recv, base=0):
        self.n, self.slot, self.send, self.recv, self.base = n_tp, slot, send, recv, base
        self.t = lax.axis_index("tp")
        if n_tp == 4:
            y, x = self.t // 2, lax.rem(self.t, 2)
            self.xn, self.yn, self.dg = y * 2 + 1 - x, (1 - y) * 2 + x, 3 - self.t

    def piece(self, owner, half, sem, to):
        ref = self.slot(owner, half)
        s = self.base + sem
        return rcopy(ref, ref, self.send.at[s], self.recv.at[s], tp=to)

    def start(self):
        if self.n == 4:
            self.piece(self.t, 0, 0, self.xn).start()
            self.piece(self.t, 1, 3, self.yn).start()
            self.piece(self.t, 1, 1, self.xn).start()
            self.piece(self.t, 0, 2, self.yn).start()
        else:
            for k in range(1, self.n):
                to = lax.rem(self.t + k, self.n)
                self.piece(self.t, None, k, to).start()

    def forward(self):
        if self.n == 4:
            self.piece(self.xn, 0, 0, self.xn).wait_recv()
            self.piece(self.xn, 0, 4, self.yn).start()
            self.piece(self.yn, 1, 3, self.yn).wait_recv()
            self.piece(self.yn, 1, 5, self.xn).start()

    def arrivals(self):
        if self.n == 4:
            self.piece(self.xn, 1, 1, self.xn).wait_recv()
            yield self.xn
            self.piece(self.yn, 0, 2, self.yn).wait_recv()
            yield self.yn
            self.piece(self.dg, 0, 4, self.yn).wait_recv()
            self.piece(self.dg, 1, 5, self.xn).wait_recv()
            yield self.dg
        else:
            for k in range(1, self.n):
                owner = lax.rem(self.t - k + self.n, self.n)
                self.piece(owner, None, k, owner).wait_recv()
                yield owner

    def drain(self):
        if self.n == 4:
            for s, half, owner in (
                (0, 0, self.t), (1, 1, self.t), (2, 0, self.t), (3, 1, self.t),
                (4, 0, self.xn), (5, 1, self.yn),
            ):
                self.piece(owner, half, s, self.xn).wait_send()
        else:
            for k in range(1, self.n):
                to = lax.rem(self.t + k, self.n)
                self.piece(self.t, None, k, to).wait_send()


def minus_expm1(y):
    series = 1.0 + y * (1 / 7.0)
    for d in (6.0, 5.0, 4.0, 3.0, 2.0):
        series = 1.0 + y * (1 / d) * series
    return jnp.where(y > -0.3, -y * series, 1.0 - jnp.exp(y))


def front_kernel(
    n_sp, n_tp,
    rec, gate, convw, wblk, base, extra, spread, perm, permt, tokens, outw, gain,
    resid, whole, normed,
    halo, cperm, gperm, av, bv, msg, totals, mixedp, mixed, squares, sqown,
    hsend, hrecv, tsend, trecv, gsend, grecv, ssend, srecv, nsend, nrecv,
):
    rows, chan = rec.shape
    groups, gw = wblk.shape[1], wblk.shape[2]
    cols = tokens.shape[1]
    seglen = rows // SEG
    sp, tp = lax.axis_index("sp"), lax.axis_index("tp")
    greet(n_sp, n_tp)
    up, down = lax.rem(sp + 1, n_sp), lax.rem(sp + n_sp - 1, n_sp)
    low = rcopy(rec.at[pl.ds(rows - 16, 16)], halo.at[0], hsend.at[0], hrecv.at[0], sp=up)
    high = rcopy(rec.at[pl.ds(0, 16)], halo.at[1], hsend.at[1], hrecv.at[1], sp=down)
    low.start()
    high.start()

    gperm[...] = jnp.dot(permt[...], gate[...], preferred_element_type=F32).astype(BF16)
    low.wait()
    high.wait()
    x = rec[...].astype(F32)
    lo = jnp.where(sp > 0, halo[0].astype(F32), 0.0)
    hi = jnp.where(sp < n_sp - 1, halo[1].astype(F32), 0.0)
    padded = jnp.concatenate([lo[14:16], x, hi[0:1]], axis=0)
    conv = padded[0:rows] * convw[0:1, :]
    for j in range(1, CONV):
        conv = conv + padded[j : j + rows] * convw[j : j + 1, :]
    cperm[...] = jnp.dot(
        permt[...], conv.astype(BF16), preferred_element_type=F32
    ).astype(BF16)

    step = 64

    @pl.loop(0, rows // step)
    def _(r):
        at = pl.ds(pl.multiple_of(r * step, step), step)
        for d in range(2):
            ex = jnp.dot(extra[d, at, :], spread[...], precision=EXACT, preferred_element_type=F32)
            for g in range(groups):
                lanes = slice(g * gw, (g + 1) * gw)
                c = cperm[at, lanes]
                rate = jax.nn.sigmoid(jnp.dot(c, wblk[2 * d, g], preferred_element_type=F32))
                admit = jax.nn.sigmoid(jnp.dot(c, wblk[2 * d + 1, g], preferred_element_type=F32))
                ld = -RATE_SCALE * rate * base[d : d + 1, lanes] + ex[:, lanes]
                bv[d, at, lanes] = jnp.sqrt(minus_expm1(2.0 * ld)) * admit * c.astype(F32)
                av[d, at, lanes] = jnp.exp(ld)

    one = jnp.ones((SEG, chan), F32)
    zero = jnp.zeros((SEG, chan), F32)

    def advance(i, carry):
        out = []
        for d in range(2):
            at = pl.ds(pl.multiple_of((i if d == 0 else seglen - 1 - i) * SEG, SEG), SEG)
            a, b = av[d, at, :], bv[d, at, :]
            cum = carry[2 * d] * a
            state = a * carry[2 * d + 1] + b
            av[d, at, :] = cum
            bv[d, at, :] = state
            out += [cum, state]
        return tuple(out)

    ends = lax.fori_loop(0, seglen, advance, (one, zero, one, zero))

    def run(d, entering):
        order = range(SEG) if d == 0 else range(SEG - 1, -1, -1)
        inside = [None] * SEG
        c = entering
        for s in order:
            inside[s] = c
            c = ends[2 * d][s : s + 1] * c + ends[2 * d + 1][s : s + 1]
        return jnp.concatenate(inside, axis=0), c

    for d in range(2):
        prod = ends[2 * d][0:1]
        for s in range(1, SEG):
            prod = prod * ends[2 * d][s : s + 1]
        msg[2 * d : 2 * d + 1, :] = prod
        msg[2 * d + 1 : 2 * d + 2, :] = run(d, jnp.zeros((1, chan), F32))[1]
    msg[4:8, :] = jnp.zeros((4, chan), F32)
    sent = []
    for k in range(1, n_sp):
        to = lax.rem(sp + k, n_sp)
        c = rcopy(msg, totals.at[k], tsend.at[k], trecv.at[k], sp=to)
        c.start()
        sent.append(c)
    for c in sent:
        c.wait()
    carries = []
    zrow = jnp.zeros((1, chan), F32)
    c0, c1 = zrow, zrow
    for k in range(n_sp - 1, 0, -1):
        t = totals[k]
        c0 = jnp.where(k <= sp, t[0:1] * c0 + t[1:2], c0)
    for k in range(1, n_sp):
        t = totals[k]
        c1 = jnp.where(k > sp, t[2:3] * c1 + t[3:4], c1)
    for d, c in ((0, c0), (1, c1)):
        inside = run(d, c)[0]
        carries.append(jnp.concatenate([inside, inside], axis=0))

    @pl.loop(0, rows // 16)
    def _(r):
        at = pl.ds(pl.multiple_of(r * 16, 16), 16)
        total = bv[0, at, :] + av[0, at, :] * carries[0]
        total = total + (bv[1, at, :] + av[1, at, :] * carries[1])
        mixedp[at, :] = (total * jax.nn.gelu(gperm[at, :].astype(F32))).astype(BF16)

    mixed[tp] = jnp.dot(perm[...], mixedp[...], preferred_element_type=F32).astype(BF16)

    half = rows // 2

    def mixed_slot(owner, part):
        return mixed.at[owner] if part is None else mixed.at[owner, pl.ds(part * half, half)]

    g = Gather(n_tp, mixed_slot, gsend, grecv)
    g.start()
    resid[...] = tokens[...].astype(F32)

    def project(owner):
        @pl.loop(0, rows // 128)
        def _(r):
            at = pl.ds(pl.multiple_of(r * 128, 128), 128)
            resid[at, :] += jnp.dot(mixed[owner, at, :], outw[owner], preferred_element_type=F32)

    project(tp)
    g.forward()
    for owner in g.arrivals():
        project(owner)

    r2 = resid[...] * resid[...]
    sqown[...] = lax.dot_general(
        jnp.ones((8, cols), F32), r2, (((1,), (1,)), ((), ())),
        precision=EXACT, preferred_element_type=F32,
    )
    sent = []
    for k in range(1, n_tp):
        c = rcopy(sqown, squares.at[k], ssend.at[k], srecv.at[k], tp=lax.rem(tp + k, n_tp))
        c.start()
        sent.append(c)
    total = sqown[...]
    for k, c in enumerate(sent):
        c.wait()
        total = total + squares[k + 1]
    scale = lax.rsqrt(total / D + NORM_EPS)
    scale = lax.dot_general(
        scale, jnp.full((8, 128), 0.125, F32), (((0,), (0,)), ((), ())),
        precision=EXACT, preferred_element_type=F32,
    )[:, 0:1]
    normed[...] = (resid[...] * scale * gain[...]).astype(BF16)
    mine = pl.ds(pl.multiple_of(tp * cols, 128), cols)
    whole[:, mine] = normed[...]

    def normed_slot(owner, part):
        lanes = pl.ds(pl.multiple_of(owner * cols, 128), cols)
        at = pl.ds(0, rows) if part is None else pl.ds(part * half, half)
        return whole.at[at, lanes]

    h = Gather(n_tp, normed_slot, nsend, nrecv)
    h.start()
    g.drain()
    h.forward()
    for owner in h.arrivals():
        pass
    h.drain()


def front(n_sp, n_tp, rec, gate, conv_weight, dw, dn, iw, inn, base, extra, tokens, outw, gain):
    rows, chan = rec.shape
    heads, wide, narrow = dw.shape[1], dw.shape[2], dn.shape[2]
    cols = tokens.shape[1]
    per = 2 if heads % 2 == 0 else 1
    hw = wide + narrow
    gw = per * hw
    blocks = []
    for d in range(2):
        for w, n in ((dw, dn), (iw, inn)):
            w = w[d].reshape(heads // per, per, wide, wide)
            n = n[d].reshape(heads // per, per, narrow, narrow)
            block = 0
            for p in range(per):
                a = p * hw
                z = ((0, 0), (a, gw - a - wide), (a, gw - a - wide))
                block = block + jnp.pad(w[:, p], z)
                a += wide
                z = ((0, 0), (a, gw - a - narrow), (a, gw - a - narrow))
                block = block + jnp.pad(n[:, p], z)
            blocks.append(block)
    wblk = jnp.stack(blocks)
    seglen = rows // SEG
    ex = extra.reshape(2, SEG, seglen, 2 * heads).swapaxes(1, 2).reshape(2, rows, 2 * heads)
    c = np.arange(chan)
    which = (c % hw >= wide) * heads + c // hw
    spread = jnp.asarray((which[None, :] == np.arange(2 * heads)[:, None]).astype(np.float32))
    r = lax.broadcasted_iota(jnp.int32, (rows, rows), 0)
    q = lax.broadcasted_iota(jnp.int32, (rows, rows), 1)
    permt = ((r % SEG) * seglen + r // SEG == q).astype(BF16)
    perm = ((q % SEG) * seglen + q // SEG == r).astype(BF16)
    vm = pl.BlockSpec(memory_space=pltpu.VMEM)
    dma = pltpu.SemaphoreType.DMA
    return pl.pallas_call(
        functools.partial(front_kernel, n_sp, n_tp),
        name="front",
        out_shape=(
            jax.ShapeDtypeStruct((rows, cols), F32),
            jax.ShapeDtypeStruct((rows, n_tp * cols), BF16),
            jax.ShapeDtypeStruct((rows, cols), BF16),
        ),
        in_specs=[vm] * 12,
        out_specs=(vm, vm, vm),
        scratch_shapes=[
            pltpu.VMEM((2, 16, chan), BF16),
            pltpu.VMEM((rows, chan), BF16),
            pltpu.VMEM((rows, chan), BF16),
            pltpu.VMEM((2, rows, chan), F32),
            pltpu.VMEM((2, rows, chan), F32),
            pltpu.VMEM((8, chan), F32),
            pltpu.VMEM((n_sp, 8, chan), F32),
            pltpu.VMEM((rows, chan), BF16),
            pltpu.VMEM((n_tp, rows, chan), BF16),
            pltpu.VMEM((n_tp, 8, rows), F32),
            pltpu.VMEM((8, rows), F32),
            dma((2,)), dma((2,)), dma((n_sp,)), dma((n_sp,)),
            *gather_sems(n_tp), dma((n_tp,)), dma((n_tp,)), *gather_sems(n_tp),
        ],
        compiler_params=pltpu.CompilerParams(
            collective_id=0, has_side_effects=True, vmem_limit_bytes=60 * 1024 * 1024
        ),
    )(
        rec, gate, conv_weight.astype(F32), wblk, base, ex, spread, perm, permt, tokens,
        outw.reshape(n_tp, chan, cols), gain.reshape(1, cols),
    )


def shards(
    rec_input,
    gate_input,
    conv_weight,
    decay_wide,
    decay_narrow,
    input_wide,
    input_narrow,
    decay_base,
    decay_extra,
    tokens,
    out_weight,
    norm_gain,
    shared_gate,
    shared_up,
    shared_down,
    expert_gate,
    expert_up,
    expert_down,
    routes,
    route_weight,
):
    seq_rows = rec_input.shape[0]
    columns = out_weight.shape[1]
    resid, whole_rows, normed = front(
        lax.axis_size("sp"), lax.axis_size("tp"), rec_input, gate_input, conv_weight,
        decay_wide, decay_narrow, input_wide, input_narrow, decay_base, decay_extra,
        tokens, out_weight, norm_gain,
    )
    width_all = whole_rows.shape[1]
    top_count = routes.shape[1]
    expert_count = lax.axis_size("sp")
    capacity = 3 * seq_rows * top_count // (2 * expert_count)
    flat_route = routes.reshape(-1)
    onehot = (flat_route[:, None] == jnp.arange(expert_count, dtype=jnp.int32)[None, :]).astype(
        jnp.int32
    )
    before = jnp.cumsum(onehot, axis=0) - onehot
    slot_ids = jnp.sum(before * onehot, axis=1)
    placing = flat_route * capacity + slot_ids
    owner_rows = jnp.arange(seq_rows * top_count, dtype=jnp.int32) // top_count
    slot_table = (
        jnp.full((expert_count * capacity,), seq_rows, jnp.int32).at[placing].set(owner_rows)
    )
    padded_cols = jnp.concatenate([normed, jnp.zeros((1, columns), jnp.bfloat16)], axis=0)
    outgoing = padded_cols[slot_table].reshape(expert_count, capacity, columns)
    arrived = lax.all_to_all(outgoing, "sp", split_axis=0, concat_axis=0, tiled=True)
    expert_rows = lax.all_gather(arrived, "tp", axis=2, tiled=True).reshape(-1, width_all)
    routed_hidden = (
        jax.nn.silu(jnp.dot(expert_rows, expert_gate[0], preferred_element_type=jnp.float32))
        * jnp.dot(expert_rows, expert_up[0], preferred_element_type=jnp.float32)
    ).astype(jnp.bfloat16)
    shared_expert_hidden = (
        jax.nn.silu(jnp.dot(whole_rows, shared_gate, preferred_element_type=jnp.float32))
        * jnp.dot(whole_rows, shared_up, preferred_element_type=jnp.float32)
    ).astype(jnp.bfloat16)
    down_local = expert_down[0]
    routed_out = jnp.dot(
        lax.all_gather(routed_hidden, "tp", axis=1, tiled=True),
        down_local,
        preferred_element_type=jnp.float32,
    )
    shared_out = jnp.dot(
        lax.all_gather(shared_expert_hidden, "tp", axis=1, tiled=True),
        shared_down,
        preferred_element_type=jnp.float32,
    )
    sending = routed_out.astype(jnp.bfloat16).reshape(expert_count, capacity, columns)
    returned = lax.all_to_all(sending, "sp", split_axis=0, concat_axis=0, tiled=True)
    picked = (
        returned.reshape(-1, columns)[placing]
        .reshape(seq_rows, top_count, columns)
        .astype(jnp.float32)
    )
    combined = jnp.sum(route_weight[:, :, None] * picked, axis=1)
    return (resid + shared_out + combined).astype(jnp.bfloat16)


def solution(mesh):
    placed = (
        P("sp", "tp"),
        P("sp", "tp"),
        P(None, "tp"),
        P(None, "tp", None, None),
        P(None, "tp", None, None),
        P(None, "tp", None, None),
        P(None, "tp", None, None),
        P(None, "tp"),
        P(None, "sp", None, "tp"),
        P("sp", "tp"),
        P(None, "tp"),
        P("tp"),
        P(None, "tp"),
        P(None, "tp"),
        P(None, "tp"),
        P("sp", None, "tp"),
        P("sp", None, "tp"),
        P("sp", None, "tp"),
        P("sp", None),
        P("sp", None),
    )
    return jax.shard_map(
        shards, mesh=mesh, in_specs=placed, out_specs=P("sp", "tp"), check_vma=False
    )
```

profile of v0, /device:TPU:0, one launch (start us, length us, event | category | flops | bytes accessed | tf_op | source)
XLA Modules:
  0.0 311.9 jit_solution(14675589117715481805)
XLA Ops:
  6.5 0.0 all-gather.6.cloned.1.call-start
  6.6 1.0 copy.45
  7.6 0.0 copy-start.4
  7.6 0.1 eq.40
  7.8 0.1 eq.36
  7.9 0.7 broadcast_multiply_fusion
  8.6 1.0 fusion.25
  9.6 1.0 fusion.26
  10.8 0.1 reshape.74
  10.9 0.9 copy.42
  11.8 0.6 convert_element_type.54.convw
  12.4 1.7 reduce-window.6
  14.1 0.1 slice.124
  14.2 0.1 copy.47
  14.3 0.2 reduce-window.9
  14.5 0.1 copy.48
  14.6 0.1 copy.44
  14.7 0.2 mul.54
  14.9 0.1 fusion.11
  15.0 3.4 %scatter_custom_fusion = s32[1152]{0:T(1024)S(1)} fusion(s32[768]{0:T(1024)S(1)} %fusion.18, s32[768]{0:T(1024)S(1)} %add_select_fusion, s32[]{:T(128)} %constant.80.clone.1), kind=kCustom, calls=%fused_computation.57 | custom fusion | bytes 4612 | tf_op jit(solution)/shard_map/scatter | solution.py:391
  18.4 0.2 add_bitcast_fusion.2
  18.6 0.2 add_bitcast_fusion
  18.8 1.8 pad_maximum_fusion.wblk
  20.6 1.2 fusion.9
  21.8 69.0 %front.1 = (f32[384,512]{1,0:T(8,128)}, bf16[384,2048]{1,0:T(8,128)(2,1)}, bf16[384,512]{1,0:T(8,128)(2,1)}) custom-call(bf16[384,768]{1,0:T(8,128)(2,1)} %rec.1, bf16[384,768]{1,0:T(8,128)(2,1)} %gate.1, f32[4,768]{1,0:T(4,128)} %convert_element_type.54.convw, bf16[4,2,384,384]{3,2,1,0:T(8,128)(2,1)} %pad_maximum_fusion.wblk, f32[2,768]{1,0:T(2,128)} %base.1, ...), custom_call_target="tpu_custom_call" | custom-call | tf_op jit(solution)/shard_map/front/pallas_call | solution.py:315
  90.8 1.0 concatenate.3
  91.8 4.7 %gather_fusion = bf16[1152,512]{1,0:T(8,128)(2,1)} fusion(bf16[385,512]{1,0:T(8,128)(2,1)S(1)} %concatenate.3, s32[2048]{0:T(1024)S(1)} %pad_clamp_fusion), kind=kCustom, calls=%fused_computation | custom fusion | bytes 2363904 | tf_op jit(solution)/shard_map/gather | solution.py:394
  96.5 33.6 %all_to_all.10 = bf16[8,144,512]{2,1,0:T(8,128)(2,1)} all-to-all(bf16[8,144,512]{2,1,0:T(8,128)(2,1)} %bitcast.120), channel_id=1, replica_groups=mesh['sp'=8,'tp'=4] {'sp'}, dimensions={0} | all-to-all | bytes 2359296 | tf_op jit(solution)/shard_map/all_to_all | solution.py:395
  130.1 0.0 all-gather.6.cloned.1.call-update
  130.2 0.2 all-gather.8.cloned.1.call-start
  130.4 54.7 %all-gather.6.cloned.1.call-done = bf16[8,144,2048]{2,1,0:T(8,128)(2,1)} async-done(((bf16[8,144,512]{2,1,0:T(8,128)(2,1)}), bf16[8,144,2048]{2,1,0:T(8,128)(2,1)}) %all-gather.6.cloned.1.call-update) | async-done | bytes 4718608 | tf_op jit(solution)/shard_map/all_gather | solution.py:396
  185.1 4.7 %fusion.3 = f32[1152,512]{1,0:T(8,128)S(1)} fusion(bf16[1152,2048]{1,0:T(8,128)(2,1)} %bitcast.135, bf16[1,2048,512]{2,1,0:T(8,128)(2,1)S(1)} %copy-done), kind=kOutput, calls=%fused_computation.9 | convolution fusion | flops 2415919104 | bytes 9175040 | tf_op jit(solution)/shard_map/dot_general | solution.py:398
  189.8 4.0 %fusion = bf16[1152,512]{1,0:T(8,128)(2,1)} fusion(bf16[1152,2048]{1,0:T(8,128)(2,1)S(1)} %bitcast.136, f32[1152,512]{1,0:T(8,128)S(1)} %fusion.3, bf16[1,2048,512]{2,1,0:T(8,128)(2,1)S(1)} %copy-done.7), kind=kOutput, calls=%fused_computation.4 | convolution fusion | flops 2419458048 | bytes 10354688 | tf_op jit(solution)/shard_map/dot_general | solution.py:399
  193.8 0.0 all-gather.8.cloned.1.call-update
  193.8 0.0 all-gather.4.cloned.1.call-start
  193.9 3.2 %fusion.29 = f32[384,512]{1,0:T(8,128)S(1)} fusion(bf16[384,2048]{1,0:T(8,128)(2,1)} %get-tuple-element.9, bf16[2048,512]{1,0:T(8,128)(2,1)} %param.33), kind=kOutput, calls=%fused_computation.76 | convolution fusion | flops 805306368 | bytes 4456448 | tf_op jit(solution)/shard_map/dot_general | solution.py:402
  197.1 1.8 fusion.6
  198.9 0.0 all-gather.4.cloned.1.call-update
  198.9 51.9 %all-gather.8.cloned.1.call-done = bf16[1152,2048]{1,0:T(8,128)(2,1)} async-done(((bf16[1152,512]{1,0:T(8,128)(2,1)}), bf16[1152,2048]{1,0:T(8,128)(2,1)}) %all-gather.8.cloned.1.call-update) | async-done | bytes 4718608 | tf_op jit(solution)/shard_map/all_gather | solution.py:407
  250.8 6.6 %convolution_convert_fusion = bf16[1152,512]{1,0:T(8,128)(2,1)} fusion(bf16[1152,2048]{1,0:T(8,128)(2,1)} %all-gather.8.cloned.1.call-done, bf16[1,2048,512]{2,1,0:T(8,128)(2,1)} %param.38), kind=kOutput, calls=%fused_computation.5 | convolution fusion | flops 2416508928 | bytes 7995392 | tf_op jit(solution)/shard_map/dot_general | solution.py:406
  257.5 4.7 %all-to-all-start.1 = ((bf16[8,144,512]{2,1,0:T(8,128)(2,1)}), bf16[8,144,512]{2,1,0:T(8,128)(2,1)S(1)}, u32[]{:S(2)}, u32[]{:S(2)}) async-start(bf16[8,144,512]{2,1,0:T(8,128)(2,1)} %bitcast.123), calls=%async_computation.1 | async-start | bytes 2359296 | tf_op jit(solution)/shard_map/all_to_all | solution.py:417
  262.2 0.1 copy.43
  262.3 29.2 %all-to-all-done.1 = bf16[8,144,512]{2,1,0:T(8,128)(2,1)S(1)} async-done(((bf16[8,144,512]{2,1,0:T(8,128)(2,1)}), bf16[8,144,512]{2,1,0:T(8,128)(2,1)S(1)}, u32[]{:S(2)}, u32[]{:S(2)}) %all-to-all-start.1) | async-done | bytes 1179680 | tf_op jit(solution)/shard_map/all_to_all | solution.py:417
  291.6 3.3 %gather_fusion.1 = bf16[768,512]{1,0:T(8,128)(2,1)} fusion(bf16[1152,512]{1,0:T(8,128)(2,1)S(1)} %bitcast.119, s32[1024]{0:T(1024)S(1)} %pad_clamp_fusion.1), kind=kCustom, calls=%fused_computation.1 | custom fusion | bytes 1575936 | tf_op jit(solution)/shard_map/gather | solution.py:419
  294.9 2.9 reshape.83
  297.8 3.6 %multiply_reduce_fusion = f32[384,512]{1,0:T(8,128)S(1)} fusion(f32[384,2,512]{2,1,0:T(2,128)} %reshape.83, f32[384,2]{1,0:T(8,128)S(1)} %copy.43), kind=kLoop, calls=%fused_computation.11 | loop fusion | flops 589824 | bytes 2362368 | tf_op jit(solution)/shard_map/reduce_sum | solution.py:423
  301.4 0.0 all-gather.4.cloned.1.call-done
  301.4 4.0 %fusion.7 = bf16[384,512]{1,0:T(8,128)(2,1)} fusion(f32[384,512]{1,0:T(8,128)S(1)} %multiply_reduce_fusion, f32[384,512]{1,0:T(8,128)} %get-tuple-element.8, bf16[384,2048]{1,0:T(8,128)(2,1)} %all-gather.4.cloned.1.call-done, bf16[2048,512]{1,0:T(8,128)(2,1)} %param.35), kind=kOutput, calls=%fused_computation.16 | convolution fusion | flops 805896192 | bytes 5636096 | tf_op jit(solution)/shard_map/dot_general | solution.py:411
  (38 shorter events, 0.2 us)
Async XLA Ops:
  6.5 178.5 %copy-start = (bf16[1,2048,512]{2,1,0:T(8,128)(2,1)S(1)}, bf16[1,2048,512]{2,1,0:T(8,128)(2,1)}, u32[]{:S(2)}) copy-start(bf16[1,2048,512]{2,1,0:T(8,128)(2,1)} %param.36) | copy-start | bytes 6291460
  6.5 4.1 %copy-start.1 = (bf16[2,4,64,64]{3,2,1,0:T(8,128)(2,1)S(1)}, bf16[2,4,64,64]{3,2,1,0:T(8,128)(2,1)}, u32[]{:S(2)}) copy-start(bf16[2,4,64,64]{3,2,1,0:T(8,128)(2,1)} %param.25) | copy-start | bytes 196612
  6.5 4.1 %copy-start.2 = (bf16[2,4,64,64]{3,2,1,0:T(8,128)(2,1)S(1)}, bf16[2,4,64,64]{3,2,1,0:T(8,128)(2,1)}, u32[]{:S(2)}) copy-start(bf16[2,4,64,64]{3,2,1,0:T(8,128)(2,1)} %param.27) | copy-start | bytes 196612
  6.5 4.2 %copy-start.3 = (f32[2,384,2,4]{1,3,2,0:T(4,128)S(1)}, f32[2,384,2,4]{1,3,2,0:T(4,128)}, u32[]{:S(2)}) copy-start(f32[2,384,2,4]{1,3,2,0:T(4,128)} %param.29) | copy-start | bytes 73732
  6.5 178.5 %all-gather.6.cloned.1.call-start = ((), (), s32[]{:S(2)}) async-start(), calls=%async_computation.3 | async-start | bytes 5898240 | tf_op jit(solution)/shard_map/all_gather | solution.py:396
  7.6 4.2 %copy-start.4 = (bf16[4,768]{1,0:T(4,128)(2,1)S(1)}, bf16[4,768]{1,0:T(4,128)(2,1)}, u32[]{:S(2)}) copy-start(bf16[4,768]{1,0:T(4,128)(2,1)} %param.23) | copy-start | bytes 18436
  130.2 120.6 %all-gather.8.cloned.1.call-start = ((), (), s32[]{:S(2)}) async-start(), calls=%async_computation.4 | async-start | bytes 5898240 | tf_op jit(solution)/shard_map/all_gather | solution.py:407
  185.1 4.7 %copy-start.6 = (bf16[8,144,2048]{2,1,0:T(8,128)(2,1)S(1)}, bf16[8,144,2048]{2,1,0:T(8,128)(2,1)}, u32[]{:S(2)}) copy-start(bf16[8,144,2048]{2,1,0:T(8,128)(2,1)} %all-gather.6.cloned.1.call-done) | copy-start | bytes 14155780
  185.1 4.7 %copy-start.7 = (bf16[1,2048,512]{2,1,0:T(8,128)(2,1)S(1)}, bf16[1,2048,512]{2,1,0:T(8,128)(2,1)}, u32[]{:S(2)}) copy-start(bf16[1,2048,512]{2,1,0:T(8,128)(2,1)} %param.37) | copy-start | bytes 6291460
  193.8 107.6 %all-gather.4.cloned.1.call-start = ((), (), s32[]{:S(2)}) async-start(), calls=%async_computation.2 | async-start | bytes 1966080 | tf_op jit(solution)/shard_map/all_gather | solution.py:412
  193.9 3.2 %copy-start.8 = (bf16[2048,512]{1,0:T(8,128)(2,1)S(1)}, bf16[2048,512]{1,0:T(8,128)(2,1)}, u32[]{:S(2)}) copy-start(bf16[2048,512]{1,0:T(8,128)(2,1)} %param.34) | copy-start | bytes 6291460
  193.9 3.2 %copy-start.9 = (bf16[384,2048]{1,0:T(8,128)(2,1)S(1)}, bf16[384,2048]{1,0:T(8,128)(2,1)}, u32[]{:S(2)}) copy-start(bf16[384,2048]{1,0:T(8,128)(2,1)} %get-tuple-element.9) | copy-start | bytes 4718596
  257.4 4.7 %copy-start.5 = (f32[384,2]{0,1:T(2,128)S(1)}, f32[384,2]{0,1:T(2,128)}, u32[]{:S(2)}) copy-start(f32[384,2]{0,1:T(2,128)} %param.40) | copy-start | bytes 9220
  257.5 34.1 %all-to-all-start.1 = ((bf16[8,144,512]{2,1,0:T(8,128)(2,1)}), bf16[8,144,512]{2,1,0:T(8,128)(2,1)S(1)}, u32[]{:S(2)}, u32[]{:S(2)}) async-start(bf16[8,144,512]{2,1,0:T(8,128)(2,1)} %bitcast.123), calls=%async_computation.1 | async-start | bytes 2359296 | tf_op jit(solution)/shard_map/all_to_all | solution.py:417
Sparse Core Ops, SparseCore 0:
  130.3 54.7 all-gather.5
  194.0 56.7 all-gather.7
  252.6 30.6 all-gather.3
where the time goes:
time: 312 us
  waiting for transfers between devices  136 us (44%)
  Pallas kernels  69 us (22%)
  blocking collectives  33.6 us (11%)
  matrix products  24.3 us (8%)
  local copies, waits for them, and re-layouts  20.5 us (7%)
  between operations  13.5 us (4%)
  other arithmetic  10.2 us (3%)
  starting transfers between devices  5.03 us (2%)
    pallas_call x1, Pallas kernels, front(): pl.pallas_call(functools.partial(front_kernel, n_sp, n_tp), name='front',...  69 us
    all_gather x1, waiting for transfers between devices, shards(): lax.all_gather(arrived, 'tp', axis=2, tiled=True).reshape(-1, width_all)  54.7 us
    all_gather x1, waiting for transfers between devices, shards(): lax.all_gather(routed_hidden, 'tp', axis=1, tiled=True)  51.9 us
    all_to_all x1, blocking collectives, shards(): lax.all_to_all(outgoing, 'sp', split_axis=0, concat_axis=0, tiled=True)  33.6 us
    all_to_all x1, waiting for transfers between devices, shards(): lax.all_to_all(sending, 'sp', split_axis=0, concat_axis=0, tiled=True)  29.2 us
    dot_general x1, matrix products, shards(): jnp.dot(lax.all_gather(routed_hidden, 'tp', axis=1, tiled=True), down_loc...  6.65 us
  transfers between devices with their start and end apart: 4, of which 3 were waited for; matrix products, arithmetic and copies ran while one was open for 7% of the time, Pallas kernels for 0%

commit v1 on v0

--- a/solution.py
+++ b/solution.py
@@ -346,6 +346,233 @@
     )
 
 
+def experts_kernel(
+    n_sp, n_tp, cap,
+    prow, pcol, weight, resid, whole, normed, hbm_sg, hbm_su, hbm_eg, hbm_eu, hbm_ed, hbm_sd,
+    out,
+    sg, su, eg, eu, ed, sd, outgoing, rows_in, hidden, answer, returned, shid, acc,
+    wsem, dsend, drecv, asend, arecv, bsend, brecv, csend, crecv, rsend, rrecv,
+):
+    rows, cols = normed.shape
+    ff = eg.shape[1]
+    sp, tp = lax.axis_index("sp"), lax.axis_index("tp")
+    count = 6 if n_tp == 4 else n_tp
+    loads = []
+    for i, (a, b) in enumerate(
+        ((hbm_sg, sg), (hbm_su, su), (hbm_eg, eg), (hbm_eu, eu), (hbm_ed, ed), (hbm_sd, sd))
+    ):
+        c = pltpu.make_async_copy(a, b, wsem.at[i])
+        c.start()
+        loads.append(c)
+    greet(n_sp, n_tp)
+
+    slot = lax.broadcasted_iota(jnp.int32, (cap, rows), 0)
+    mine = pl.ds(pl.multiple_of(tp * cols, 128), cols)
+    fmine = pl.ds(pl.multiple_of(tp * ff, 128), ff)
+
+    def dispatch(k):
+        to = lax.rem(sp + k, n_sp)
+        return rcopy(
+            outgoing.at[to], rows_in.at[sp, :, mine], dsend.at[k], drecv.at[k], sp=to
+        )
+
+    def landed(k):
+        src = lax.rem(sp - k + n_sp, n_sp)
+        return rcopy(
+            outgoing.at[src], rows_in.at[src, :, mine], dsend.at[k], drecv.at[k], sp=src
+        )
+
+    def reply(k):
+        src = lax.rem(sp - k + n_sp, n_sp)
+        return rcopy(answer.at[src], returned.at[sp], rsend.at[k], rrecv.at[k], sp=src)
+
+    def replied(k):
+        e = lax.rem(sp + k, n_sp)
+        return rcopy(answer.at[e], returned.at[e], rsend.at[k], rrecv.at[k], sp=e)
+
+    @pl.loop(0, n_sp)
+    def _(k):
+        e = lax.rem(sp + k, n_sp)
+        hit = (prow[0:1, :] - e * cap == slot) | (prow[1:2, :] - e * cap == slot)
+        picked = jnp.dot(
+            hit.astype(F32).astype(BF16), normed[...], preferred_element_type=F32
+        ).astype(BF16)
+
+        @pl.when(k == 0)
+        def _():
+            rows_in[sp, :, mine] = picked
+
+        @pl.when(k > 0)
+        def _():
+            outgoing[e] = picked
+            dispatch(k).start()
+
+    def gather(buffer, width, send, recv, k):
+        src = lax.rem(sp - k + n_sp, n_sp)
+
+        def place(owner, part):
+            if part is None:
+                return buffer.at[src, :, pl.ds(pl.multiple_of(owner * width, 128), width)]
+            half = width // 2
+            first = pl.multiple_of(owner * width + part * half, 128)
+            return buffer.at[src, :, pl.ds(first, half)]
+
+        return Gather(n_tp, place, send, recv, base=k * count)
+
+    def rows_gather(k):
+        return gather(rows_in, cols, asend, arecv, k)
+
+    def hidden_gather(k):
+        return gather(hidden, ff, bsend, brecv, k)
+
+    def shared_place(owner, part):
+        if part is None:
+            return shid.at[:, pl.ds(pl.multiple_of(owner * ff, 128), ff)]
+        half = ff // 2
+        first = pl.multiple_of(owner * ff + part * half, 128)
+        return shid.at[:, pl.ds(first, half)]
+
+    shared = Gather(n_tp, shared_place, csend, crecv)
+    rows_gather(0).start()
+    loads[0].wait()
+    loads[1].wait()
+
+    @pl.loop(0, rows // 128)
+    def _(r):
+        at = pl.ds(pl.multiple_of(r * 128, 128), 128)
+        x = whole[at, :]
+        g = jnp.dot(x, sg[...], preferred_element_type=F32)
+        u = jnp.dot(x, su[...], preferred_element_type=F32)
+        shid[at, fmine] = (jax.nn.silu(g) * u).astype(BF16)
+
+    for c in loads[2:5]:
+        c.wait()
+
+    @pl.loop(0, n_sp + 4)
+    def _(step):
+        @pl.when((step > 0) & (step < n_sp))
+        def _():
+            landed(step).wait_recv()
+            rows_gather(step).start()
+
+        @pl.when((step >= 1) & (step < n_sp + 1))
+        def _():
+            rows_gather(step - 1).forward()
+
+        @pl.when((step >= 2) & (step < n_sp + 2))
+        def _():
+            k = step - 2
+            src = lax.rem(sp - k + n_sp, n_sp)
+            for _ in rows_gather(k).arrivals():
+                pass
+            x = rows_in[src]
+            g = jnp.dot(x, eg[...], preferred_element_type=F32)
+            u = jnp.dot(x, eu[...], preferred_element_type=F32)
+            hidden[src, :, fmine] = (jax.nn.silu(g) * u).astype(BF16)
+            hidden_gather(k).start()
+
+        @pl.when(step == n_sp + 1)
+        def _():
+            shared.start()
+
+        @pl.when((step >= 3) & (step < n_sp + 3))
+        def _():
+            hidden_gather(step - 3).forward()
+
+        @pl.when(step >= 4)
+        def _():
+            k = step - 4
+            src = lax.rem(sp - k + n_sp, n_sp)
+            for _ in hidden_gather(k).arrivals():
+                pass
+            y = jnp.dot(hidden[src], ed[...], preferred_element_type=F32).astype(BF16)
+
+            @pl.when(k == 0)
+            def _():
+                returned[sp] = y
+
+            @pl.when(k > 0)
+            def _():
+                answer[src] = y
+                reply(k).start()
+
+    shared.forward()
+    loads[5].wait()
+    for _ in shared.arrivals():
+        pass
+
+    @pl.loop(0, rows // 128)
+    def _(r):
+        at = pl.ds(pl.multiple_of(r * 128, 128), 128)
+        acc[at, :] = resid[at, :] + jnp.dot(shid[at, :], sd[...], preferred_element_type=F32)
+
+    @pl.loop(0, n_sp)
+    def _(k):
+        e = lax.rem(sp + k, n_sp)
+
+        @pl.when(k > 0)
+        def _():
+            replied(k).wait_recv()
+
+        lane = lax.broadcasted_iota(jnp.int32, (128, cap), 1)
+
+        @pl.loop(0, rows // 128)
+        def _(r):
+            at = pl.ds(pl.multiple_of(r * 128, 128), 128)
+            p0 = pcol[at, 0:1] - e * cap
+            p1 = pcol[at, 1:2] - e * cap
+            w = jnp.where((p0 >= 0) & (p0 < cap), weight[at, 0:1], 0.0) + jnp.where(
+                (p1 >= 0) & (p1 < cap), weight[at, 1:2], 0.0
+            )
+            hit = ((p0 == lane) | (p1 == lane)).astype(F32).astype(BF16)
+            acc[at, :] += w * jnp.dot(hit, returned[e], preferred_element_type=F32)
+
+    out[...] = acc[...].astype(BF16)
+    shared.drain()
+
+    @pl.loop(0, n_sp)
+    def _(k):
+        rows_gather(k).drain()
+        hidden_gather(k).drain()
+
+        @pl.when(k > 0)
+        def _():
+            dispatch(k).wait_send()
+            reply(k).wait_send()
+
+
+def experts(n_sp, n_tp, cap, placing, route_weight, resid, whole, normed, weights):
+    rows, cols = normed.shape
+    ff = weights[0].shape[1]
+    vm = pl.BlockSpec(memory_space=pltpu.VMEM)
+    hbm = pl.BlockSpec(memory_space=pl.ANY)
+    dma = pltpu.SemaphoreType.DMA
+    count = 6 if n_tp == 4 else n_tp
+    return pl.pallas_call(
+        functools.partial(experts_kernel, n_sp, n_tp, cap),
+        name="experts",
+        out_shape=jax.ShapeDtypeStruct((rows, cols), BF16),
+        in_specs=[vm] * 6 + [hbm] * 6,
+        out_specs=vm,
+        scratch_shapes=[pltpu.VMEM(w.shape, BF16) for w in weights] + [
+            pltpu.VMEM((n_sp, cap, cols), BF16),
+            pltpu.VMEM((n_sp, cap, n_tp * cols), BF16),
+            pltpu.VMEM((n_sp, cap, n_tp * ff), BF16),
+            pltpu.VMEM((n_sp, cap, cols), BF16),
+            pltpu.VMEM((n_sp, cap, cols), BF16),
+            pltpu.VMEM((rows, n_tp * ff), BF16),
+            pltpu.VMEM((rows, cols), F32),
+            dma((6,)), dma((n_sp,)), dma((n_sp,)),
+            dma((n_sp * count,)), dma((n_sp * count,)),
+            dma((n_sp * count,)), dma((n_sp * count,)),
+            *gather_sems(n_tp), dma((n_sp,)), dma((n_sp,)),
+        ],
+        compiler_params=pltpu.CompilerParams(
+            collective_id=1, has_side_effects=True, vmem_limit_bytes=60 * 1024 * 1024
+        ),
+    )(placing.T, placing, route_weight, resid, whole, normed, *weights)
+
+
 def shards(
     rec_input,
     gate_input,
@@ -375,7 +602,6 @@
         decay_wide, decay_narrow, input_wide, input_narrow, decay_base, decay_extra,
         tokens, out_weight, norm_gain,
     )
-    width_all = whole_rows.shape[1]
     top_count = routes.shape[1]
     expert_count = lax.axis_size("sp")
     capacity = 3 * seq_rows * top_count // (2 * expert_count)
@@ -385,43 +611,11 @@
     )
     before = jnp.cumsum(onehot, axis=0) - onehot
     slot_ids = jnp.sum(before * onehot, axis=1)
-    placing = flat_route * capacity + slot_ids
-    owner_rows = jnp.arange(seq_rows * top_count, dtype=jnp.int32) // top_count
-    slot_table = (
-        jnp.full((expert_count * capacity,), seq_rows, jnp.int32).at[placing].set(owner_rows)
-    )
-    padded_cols = jnp.concatenate([normed, jnp.zeros((1, columns), jnp.bfloat16)], axis=0)
-    outgoing = padded_cols[slot_table].reshape(expert_count, capacity, columns)
-    arrived = lax.all_to_all(outgoing, "sp", split_axis=0, concat_axis=0, tiled=True)
-    expert_rows = lax.all_gather(arrived, "tp", axis=2, tiled=True).reshape(-1, width_all)
-    routed_hidden = (
-        jax.nn.silu(jnp.dot(expert_rows, expert_gate[0], preferred_element_type=jnp.float32))
-        * jnp.dot(expert_rows, expert_up[0], preferred_element_type=jnp.float32)
-    ).astype(jnp.bfloat16)
-    shared_expert_hidden = (
-        jax.nn.silu(jnp.dot(whole_rows, shared_gate, preferred_element_type=jnp.float32))
-        * jnp.dot(whole_rows, shared_up, preferred_element_type=jnp.float32)
-    ).astype(jnp.bfloat16)
-    down_local = expert_down[0]
-    routed_out = jnp.dot(
-        lax.all_gather(routed_hidden, "tp", axis=1, tiled=True),
-        down_local,
-        preferred_element_type=jnp.float32,
-    )
-    shared_out = jnp.dot(
-        lax.all_gather(shared_expert_hidden, "tp", axis=1, tiled=True),
-        shared_down,
-        preferred_element_type=jnp.float32,
-    )
-    sending = routed_out.astype(jnp.bfloat16).reshape(expert_count, capacity, columns)
-    returned = lax.all_to_all(sending, "sp", split_axis=0, concat_axis=0, tiled=True)
-    picked = (
-        returned.reshape(-1, columns)[placing]
-        .reshape(seq_rows, top_count, columns)
-        .astype(jnp.float32)
-    )
-    combined = jnp.sum(route_weight[:, :, None] * picked, axis=1)
-    return (resid + shared_out + combined).astype(jnp.bfloat16)
+    placing = (flat_route * capacity + slot_ids).reshape(seq_rows, top_count)
+    return experts(
+        expert_count, lax.axis_size("tp"), capacity, placing, route_weight, resid, whole_rows, normed,
+        (shared_gate, shared_up, expert_gate[0], expert_up[0], expert_down[0], shared_down),
+    )
 
 
 def solution(mesh):

time: 312 us -> 192 us (0.62)
  waiting for transfers between devices: 136 us -> 0 us
  Pallas kernels: 69 us -> 178 us
  blocking collectives: 33.6 us -> 0 us
  matrix products: 24.3 us -> 0 us
  between operations: 13.5 us -> 0.24 us
  local copies, waits for them, and re-layouts: 20.5 us -> 7.47 us
  starting transfers between devices: 5.03 us -> 0 us
  other arithmetic: 10.2 us -> 6.06 us
    pallas_call x0 -> x1, Pallas kernels: none -> 109 us  [experts(): pl.pallas_call(functools.partial(experts_kernel, n_sp, n_tp, cap), name='...]
    all_gather x3 -> x0, waiting for transfers between devices: 107 us -> none  [the longest x1 54.7 us: shards(): lax.all_gather(arrived, 'tp', axis=2, tiled=True).reshape(-1, width_all)]
    all_to_all x1 -> x0, blocking collectives: 33.6 us -> none  [shards(): lax.all_to_all(outgoing, 'sp', split_axis=0, concat_axis=0, tiled=True)]
    all_to_all x1 -> x0, waiting for transfers between devices: 29.2 us -> none  [shards(): lax.all_to_all(sending, 'sp', split_axis=0, concat_axis=0, tiled=True)]
    dot_general x6 -> x0, matrix products: 24.3 us -> none  [the longest x1 6.65 us: shards(): jnp.dot(lax.all_gather(routed_hidden, 'tp', axis=1, tiled=True), down_loc...]
    gather x2 -> x0, local copies, waits for them, and re-layouts: 8 us -> none  [the longest x1 4.68 us: shards(): outgoing = padded_cols[slot_table].reshape(expert_count, capacity, columns)]
    all_to_all x1 -> x0, starting transfers between devices: 4.73 us -> none  [shards(): lax.all_to_all(sending, 'sp', split_axis=0, concat_axis=0, tiled=True)]
    reduce_sum x1 -> x0, other arithmetic: 3.56 us -> none  [shards(): combined = jnp.sum(route_weight[:, :, None] * picked, axis=1)]
  transfers between devices with their start and end apart: 4 -> 0, of which waited for: 3 -> 0; matrix products, arithmetic and copies ran while one was open for 7% -> 0% of each run, Pallas kernels for 0% -> 0%
where the time goes in v1:
time: 192 us
  Pallas kernels  178 us (93%)
  local copies, waits for them, and re-layouts  7.47 us (4%)
  other arithmetic  6.06 us (3%)
    pallas_call x1, Pallas kernels, experts(): pl.pallas_call(functools.partial(experts_kernel, n_sp, n_tp, cap), name='...  109 us
    pallas_call x1, Pallas kernels, front(): pl.pallas_call(functools.partial(front_kernel, n_sp, n_tp), name='front',...  68.9 us

profile of v1, /device:TPU:0, one launch (start us, length us, event | category | flops | bytes accessed | tf_op | source)
XLA Modules:
  0.0 191.9 jit_solution(3798772843154833682)
XLA Ops:
  0.0 0.0 copy-start.1
  0.0 0.0 copy-start.2
  0.0 1.0 fusion.11
  1.1 1.0 fusion.12
  2.1 0.0 copy-done.1
  2.1 0.0 copy-done.2
  2.2 0.2 add_bitcast_fusion.2
  2.4 0.2 add_bitcast_fusion
  2.6 0.0 copy-start.3
  2.6 1.8 pad_maximum_fusion.wblk
  4.4 0.0 copy-start.5
  4.5 1.3 fusion.1
  5.7 0.0 copy-done.3
  5.7 0.1 reshape.33
  5.8 0.9 copy.75
  6.8 0.0 copy-done.5
  6.8 0.6 convert_element_type.38.convw
  7.4 0.0 copy-start.4
  7.4 68.9 %front.1 = (f32[384,512]{1,0:T(8,128)}, bf16[384,2048]{1,0:T(8,128)(2,1)}, bf16[384,512]{1,0:T(8,128)(2,1)}) custom-call(bf16[384,768]{1,0:T(8,128)(2,1)} %rec.1, bf16[384,768]{1,0:T(8,128)(2,1)} %gate.1, f32[4,768]{1,0:T(4,128)} %convert_element_type.38.convw, bf16[4,2,384,384]{3,2,1,0:T(8,128)(2,1)} %pad_maximum_fusion.wblk, f32[2,768]{1,0:T(2,128)} %base.1, ...), custom_call_target="tpu_custom_call" | custom-call | tf_op jit(solution)/shard_map/front/pallas_call | solution.py:315
  76.3 0.0 copy-start.6
  76.3 0.0 copy-done.4
  76.3 0.1 copy.54
  76.4 0.1 eq.38
  76.6 1.7 reduce-window.6
  78.3 0.1 slice.104
  78.4 0.1 copy.56
  78.5 0.2 reduce-window.9
  78.7 0.1 copy.57
  78.8 0.1 eq.34
  78.9 0.1 fusion.3
  79.0 0.2 reduce_sum.12
  79.2 0.1 copy.58
  79.4 0.0 copy-start
  79.4 0.7 copy.76.prow
  80.1 0.0 copy-done.6
  80.1 0.8 copy.77.weight
  80.9 0.0 copy-done
  80.9 109.3 %experts.1 = bf16[384,512]{1,0:T(8,128)(2,1)} custom-call(s32[2,384]{1,0:T(2,128)} %copy.76.prow, s32[384,2]{1,0:T(8,128)} %copy-done, f32[384,2]{1,0:T(8,128)} %copy.77.weight, f32[384,512]{1,0:T(8,128)} %get-tuple-element.8.resid, bf16[384,2048]{1,0:T(8,128)(2,1)} %get-tuple-element.9.whole, bf16[384,512]{1,0:T(8,128)(2,1)} %get-tuple-element.10.normed, ...), custom_call_target="tpu_custom_call" | custom-call | tf_op jit(solution)/shard_map/experts/pallas_call | solution.py:551
  190.2 1.8 copy.95
  (16 shorter events, 0.1 us)
Async XLA Ops:
  0.0 2.1 %copy-start.1 = (bf16[2,4,64,64]{3,2,1,0:T(8,128)(2,1)S(1)}, bf16[2,4,64,64]{3,2,1,0:T(8,128)(2,1)}, u32[]{:S(2)}) copy-start(bf16[2,4,64,64]{3,2,1,0:T(8,128)(2,1)} %param.25) | copy-start | bytes 196612
  0.0 2.1 %copy-start.2 = (bf16[2,4,64,64]{3,2,1,0:T(8,128)(2,1)S(1)}, bf16[2,4,64,64]{3,2,1,0:T(8,128)(2,1)}, u32[]{:S(2)}) copy-start(bf16[2,4,64,64]{3,2,1,0:T(8,128)(2,1)} %param.27) | copy-start | bytes 196612
  2.6 3.1 %copy-start.3 = (f32[2,384,2,4]{1,3,2,0:T(4,128)S(1)}, f32[2,384,2,4]{1,3,2,0:T(4,128)}, u32[]{:S(2)}) copy-start(f32[2,384,2,4]{1,3,2,0:T(4,128)} %param.29) | copy-start | bytes 73732
  4.4 2.3 %copy-start.5 = (bf16[4,768]{1,0:T(4,128)(2,1)S(1)}, bf16[4,768]{1,0:T(4,128)(2,1)}, u32[]{:S(2)}) copy-start(bf16[4,768]{1,0:T(4,128)(2,1)} %param.23) | copy-start | bytes 18436
  7.4 68.9 %copy-start.4 = (s32[384,2]{0,1:T(2,128)S(1)}, s32[384,2]{0,1:T(2,128)}, u32[]{:S(2)}) copy-start(s32[384,2]{0,1:T(2,128)} %param.39) | copy-start | bytes 9220
  76.3 3.8 %copy-start.6 = (f32[384,2]{0,1:T(2,128)S(1)}, f32[384,2]{0,1:T(2,128)}, u32[]{:S(2)}) copy-start(f32[384,2]{0,1:T(2,128)} %param.40) | copy-start | bytes 9220
  79.4 1.5 copy-start

commit v2 on v1

--- a/solution.py
+++ b/solution.py
@@ -112,16 +112,18 @@
 
 def front_kernel(
     n_sp, n_tp,
-    rec, gate, convw, wblk, base, extra, spread, perm, permt, tokens, outw, gain,
+    rec, gate, convw, wblk, base, extra, spread, perm, permt, tokens, hbm_outw, gain,
     resid, whole, normed,
     halo, cperm, gperm, av, bv, msg, totals, mixedp, mixed, squares, sqown,
-    hsend, hrecv, tsend, trecv, gsend, grecv, ssend, srecv, nsend, nrecv,
+    hsend, hrecv, tsend, trecv, gsend, grecv, ssend, srecv, nsend, nrecv, outw, wsem,
 ):
     rows, chan = rec.shape
     groups, gw = wblk.shape[1], wblk.shape[2]
     cols = tokens.shape[1]
     seglen = rows // SEG
     sp, tp = lax.axis_index("sp"), lax.axis_index("tp")
+    load = pltpu.make_async_copy(hbm_outw, outw, wsem.at[0])
+    load.start()
     greet(n_sp, n_tp)
     up, down = lax.rem(sp + 1, n_sp), lax.rem(sp + n_sp - 1, n_sp)
     low = rcopy(rec.at[pl.ds(rows - 16, 16)], halo.at[0], hsend.at[0], hrecv.at[0], sp=up)
@@ -237,6 +239,7 @@
             at = pl.ds(pl.multiple_of(r * 128, 128), 128)
             resid[at, :] += jnp.dot(mixed[owner, at, :], outw[owner], preferred_element_type=F32)
 
+    load.wait()
     project(tp)
     g.forward()
     for owner in g.arrivals():
@@ -320,7 +323,7 @@
             jax.ShapeDtypeStruct((rows, n_tp * cols), BF16),
             jax.ShapeDtypeStruct((rows, cols), BF16),
         ),
-        in_specs=[vm] * 12,
+        in_specs=[vm] * 10 + [pl.BlockSpec(memory_space=pl.ANY), vm],
         out_specs=(vm, vm, vm),
         scratch_shapes=[
             pltpu.VMEM((2, 16, chan), BF16),
@@ -336,6 +339,7 @@
             pltpu.VMEM((8, rows), F32),
             dma((2,)), dma((2,)), dma((n_sp,)), dma((n_sp,)),
             *gather_sems(n_tp), dma((n_tp,)), dma((n_tp,)), *gather_sems(n_tp),
+            pltpu.VMEM((n_tp, chan, cols), BF16), dma((1,)),
         ],
         compiler_params=pltpu.CompilerParams(
             collective_id=0, has_side_effects=True, vmem_limit_bytes=60 * 1024 * 1024
@@ -445,69 +449,11 @@
         u = jnp.dot(x, su[...], preferred_element_type=F32)
         shid[at, fmine] = (jax.nn.silu(g) * u).astype(BF16)
 
+    shared.start()
     for c in loads[2:5]:
         c.wait()
 
-    @pl.loop(0, n_sp + 4)
-    def _(step):
-        @pl.when((step > 0) & (step < n_sp))
-        def _():
-            landed(step).wait_recv()
-            rows_gather(step).start()
-
-        @pl.when((step >= 1) & (step < n_sp + 1))
-        def _():
-            rows_gather(step - 1).forward()
-
-        @pl.when((step >= 2) & (step < n_sp + 2))
-        def _():
-            k = step - 2
-            src = lax.rem(sp - k + n_sp, n_sp)
-            for _ in rows_gather(k).arrivals():
-                pass
-            x = rows_in[src]
-            g = jnp.dot(x, eg[...], preferred_element_type=F32)
-            u = jnp.dot(x, eu[...], preferred_element_type=F32)
-            hidden[src, :, fmine] = (jax.nn.silu(g) * u).astype(BF16)
-            hidden_gather(k).start()
-
-        @pl.when(step == n_sp + 1)
-        def _():
-            shared.start()
-
-        @pl.when((step >= 3) & (step < n_sp + 3))
-        def _():
-            hidden_gather(step - 3).forward()
-
-        @pl.when(step >= 4)
-        def _():
-            k = step - 4
-            src = lax.rem(sp - k + n_sp, n_sp)
-            for _ in hidden_gather(k).arrivals():
-                pass
-            y = jnp.dot(hidden[src], ed[...], preferred_element_type=F32).astype(BF16)
-
-            @pl.when(k == 0)
-            def _():
-                returned[sp] = y
-
-            @pl.when(k > 0)
-            def _():
-                answer[src] = y
-                reply(k).start()
-
-    shared.forward()
-    loads[5].wait()
-    for _ in shared.arrivals():
-        pass
-
-    @pl.loop(0, rows // 128)
-    def _(r):
-        at = pl.ds(pl.multiple_of(r * 128, 128), 128)
-        acc[at, :] = resid[at, :] + jnp.dot(shid[at, :], sd[...], preferred_element_type=F32)
-
-    @pl.loop(0, n_sp)
-    def _(k):
+    def combine(k):
         e = lax.rem(sp + k, n_sp)
 
         @pl.when(k > 0)
@@ -526,6 +472,75 @@
             )
             hit = ((p0 == lane) | (p1 == lane)).astype(F32).astype(BF16)
             acc[at, :] += w * jnp.dot(hit, returned[e], preferred_element_type=F32)
+
+    @pl.loop(0, n_sp + 4)
+    def _(step):
+        @pl.when((step > 0) & (step < n_sp))
+        def _():
+            landed(step).wait_recv()
+            rows_gather(step).start()
+
+        @pl.when((step >= 1) & (step < n_sp + 1))
+        def _():
+            rows_gather(step - 1).forward()
+
+        @pl.when((step >= 2) & (step < n_sp + 2))
+        def _():
+            k = step - 2
+            src = lax.rem(sp - k + n_sp, n_sp)
+            for _ in rows_gather(k).arrivals():
+                pass
+            x = rows_in[src]
+            g = jnp.dot(x, eg[...], preferred_element_type=F32)
+            u = jnp.dot(x, eu[...], preferred_element_type=F32)
+            hidden[src, :, fmine] = (jax.nn.silu(g) * u).astype(BF16)
+            hidden_gather(k).start()
+
+        @pl.when(step == 1)
+        def _():
+            shared.forward()
+
+        @pl.when(step == 4)
+        def _():
+            loads[5].wait()
+            for _ in shared.arrivals():
+                pass
+
+            @pl.loop(0, rows // 128)
+            def _(r):
+                at = pl.ds(pl.multiple_of(r * 128, 128), 128)
+                acc[at, :] = resid[at, :] + jnp.dot(
+                    shid[at, :], sd[...], preferred_element_type=F32
+                )
+
+        @pl.when(step >= 6)
+        def _():
+            combine(step - 6)
+
+        @pl.when((step >= 3) & (step < n_sp + 3))
+        def _():
+            hidden_gather(step - 3).forward()
+
+        @pl.when(step >= 4)
+        def _():
+            k = step - 4
+            src = lax.rem(sp - k + n_sp, n_sp)
+            for _ in hidden_gather(k).arrivals():
+                pass
+            y = jnp.dot(hidden[src], ed[...], preferred_element_type=F32).astype(BF16)
+
+            @pl.when(k == 0)
+            def _():
+                returned[sp] = y
+
+            @pl.when(k > 0)
+            def _():
+                answer[src] = y
+                reply(k).start()
+
+    @pl.loop(n_sp - 2, n_sp)
+    def _(k):
+        combine(k)
 
     out[...] = acc[...].astype(BF16)
     shared.drain()

time: 192 us -> 188 us (0.979)
  Pallas kernels: 178 us -> 174 us
    pallas_call x1, Pallas kernels: 109 us -> 107 us  [experts(): pl.pallas_call(functools.partial(experts_kernel, n_sp, n_tp, cap), name='...]
where the time goes in v2:
time: 188 us
  Pallas kernels  174 us (93%)
  local copies, waits for them, and re-layouts  7.47 us (4%)
  other arithmetic  6.06 us (3%)
    pallas_call x1, Pallas kernels, experts(): pl.pallas_call(functools.partial(experts_kernel, n_sp, n_tp, cap), name='...  107 us
    pallas_call x1, Pallas kernels, front(): pl.pallas_call(functools.partial(front_kernel, n_sp, n_tp), name='front',...  67.8 us

profile of v2, /device:TPU:0, one launch (start us, length us, event | category | flops | bytes accessed | tf_op | source)
XLA Modules:
  0.0 188.2 jit_solution(12927821856471493654)
XLA Ops:
  0.0 0.0 copy-start.1
  0.0 0.0 copy-start.2
  0.0 1.0 fusion.11
  1.1 1.0 fusion.12
  2.1 0.0 copy-done.1
  2.1 0.0 copy-done.2
  2.2 0.2 add_bitcast_fusion.2
  2.4 0.2 add_bitcast_fusion
  2.6 0.0 copy-start.3
  2.6 1.8 pad_maximum_fusion.wblk
  4.4 0.0 copy-start.5
  4.5 1.3 fusion.1
  5.7 0.0 copy-done.3
  5.7 0.1 reshape.33
  5.8 0.9 copy.75
  6.8 0.0 copy-done.5
  6.8 0.6 convert_element_type.38.convw
  7.4 0.0 copy-start.4
  7.4 67.8 %front.1 = (f32[384,512]{1,0:T(8,128)}, bf16[384,2048]{1,0:T(8,128)(2,1)}, bf16[384,512]{1,0:T(8,128)(2,1)}) custom-call(bf16[384,768]{1,0:T(8,128)(2,1)} %rec.1, bf16[384,768]{1,0:T(8,128)(2,1)} %gate.1, f32[4,768]{1,0:T(4,128)} %convert_element_type.38.convw, bf16[4,2,384,384]{3,2,1,0:T(8,128)(2,1)} %pad_maximum_fusion.wblk, f32[2,768]{1,0:T(2,128)} %base.1, ...), custom_call_target="tpu_custom_call" | custom-call | tf_op jit(solution)/shard_map/front/pallas_call | solution.py:318
  75.2 0.0 copy-start.6
  75.2 0.0 copy-done.4
  75.2 0.1 copy.54
  75.4 0.1 eq.38
  75.5 1.7 reduce-window.6
  77.3 0.1 slice.104
  77.3 0.1 copy.56
  77.5 0.2 reduce-window.9
  77.6 0.1 copy.57
  77.7 0.1 eq.34
  77.9 0.1 fusion.3
  78.0 0.2 reduce_sum.12
  78.1 0.1 copy.58
  78.3 0.0 copy-start
  78.3 0.7 copy.76.prow
  79.0 0.0 copy-done.6
  79.0 0.8 copy.77.weight
  79.8 0.0 copy-done
  79.9 106.6 %experts.1 = bf16[384,512]{1,0:T(8,128)(2,1)} custom-call(s32[2,384]{1,0:T(2,128)} %copy.76.prow, s32[384,2]{1,0:T(8,128)} %copy-done, f32[384,2]{1,0:T(8,128)} %copy.77.weight, f32[384,512]{1,0:T(8,128)} %get-tuple-element.8.resid, bf16[384,2048]{1,0:T(8,128)(2,1)} %get-tuple-element.9.whole, bf16[384,512]{1,0:T(8,128)(2,1)} %get-tuple-element.10.normed, ...), custom_call_target="tpu_custom_call" | custom-call | tf_op jit(solution)/shard_map/experts/pallas_call | solution.py:566
  186.4 1.8 copy.95
  (16 shorter events, 0.1 us)
Async XLA Ops:
  0.0 2.1 %copy-start.1 = (bf16[2,4,64,64]{3,2,1,0:T(8,128)(2,1)S(1)}, bf16[2,4,64,64]{3,2,1,0:T(8,128)(2,1)}, u32[]{:S(2)}) copy-start(bf16[2,4,64,64]{3,2,1,0:T(8,128)(2,1)} %param.25) | copy-start | bytes 196612
  0.0 2.1 %copy-start.2 = (bf16[2,4,64,64]{3,2,1,0:T(8,128)(2,1)S(1)}, bf16[2,4,64,64]{3,2,1,0:T(8,128)(2,1)}, u32[]{:S(2)}) copy-start(bf16[2,4,64,64]{3,2,1,0:T(8,128)(2,1)} %param.27) | copy-start | bytes 196612
  2.6 3.1 %copy-start.3 = (f32[2,384,2,4]{1,3,2,0:T(4,128)S(1)}, f32[2,384,2,4]{1,3,2,0:T(4,128)}, u32[]{:S(2)}) copy-start(f32[2,384,2,4]{1,3,2,0:T(4,128)} %param.29) | copy-start | bytes 73732
  4.4 2.3 %copy-start.5 = (bf16[4,768]{1,0:T(4,128)(2,1)S(1)}, bf16[4,768]{1,0:T(4,128)(2,1)}, u32[]{:S(2)}) copy-start(bf16[4,768]{1,0:T(4,128)(2,1)} %param.23) | copy-start | bytes 18436
  7.4 67.9 %copy-start.4 = (s32[384,2]{0,1:T(2,128)S(1)}, s32[384,2]{0,1:T(2,128)}, u32[]{:S(2)}) copy-start(s32[384,2]{0,1:T(2,128)} %param.39) | copy-start | bytes 9220
  75.2 3.8 %copy-start.6 = (f32[384,2]{0,1:T(2,128)S(1)}, f32[384,2]{0,1:T(2,128)}, u32[]{:S(2)}) copy-start(f32[384,2]{0,1:T(2,128)} %param.40) | copy-start | bytes 9220
  78.3 1.5 copy-start
